TPU v7x, 32 devices: a whole 2x2x4 slice. The times are simulated.
32 devices in a mesh: sp: 8 (over z, y), tp: 4 (over x, core).
Axes of the slice: x: 2, y: 2, z: 4, core: 2. Of those that a mesh axis runs over, the one named last changes fastest.
Arguments:
- frames: bfloat16 [4, 1024, 1024], P('tp', 'sp'), may hold values from -22 to 22
- norm_gain: float32 [1024], replicated, may hold values from 0.5 to 1.5
- conv_value_w: bfloat16 [1024, 512], P(None, 'tp'), may hold values from -0.1875 to 0.1875
- conv_gate_w: bfloat16 [1024, 512], P(None, 'tp'), may hold values from -0.1875 to 0.1875
- conv_taps: bfloat16 [31, 512], P(None, 'tp'), may hold values from -1 to 1
- conv_bias: float32 [512], P('tp'), may hold values from -1.2 to 1.2
- channel_gain: float32 [512], P('tp'), may hold values from 0.5 to 1.5
- channel_shift: float32 [512], P('tp'), may hold values from -1.2 to 1.2
- query_w: bfloat16 [1024, 1024], P(None, 'tp'), may hold values from -0.1875 to 0.1875
- forget_w: bfloat16 [1024, 1024], P(None, 'tp'), may hold values from -0.1875 to 0.1875
- input_w: bfloat16 [1024, 1024], P(None, 'tp'), may hold values from -0.1875 to 0.1875
- gate_w: bfloat16 [1024, 1024], P(None, 'tp'), may hold values from -0.1875 to 0.1875
- memory_rate: float32 [1024], P('tp'), may hold values from 0.5 to 32
- head_gain: float32 [1024], P('tp'), may hold values from 0.5 to 1.5
- conv_out_w: bfloat16 [512, 1024], P('tp'), may hold values from -0.1875 to 0.1875
- rec_out_w: bfloat16 [1024, 1024], P('tp'), may hold values from -0.125 to 0.125
Outputs:
- mixed: bfloat16 [4, 1024, 1024], P('tp', 'sp')
All inputs are finite; a program needn't handle non-finite values.
Results may differ from a plain program's by a relative error of at most 0.015.
The roundings to bfloat16 on the way count: a program that leaves them out, or rounds other values in their place, can miss the bound.
Values may be sent and summed in bfloat16 or wider, within the bound.
A program may use at most 64 MiB of HBM per device.

v0:
```python
import jax
import jax.numpy as jnp
from jax import lax
from jax.sharding import PartitionSpec as P

D_CONV = 512
HEAD = 128


EPS = 1e-06


def from_behind(value, axis, steps):
    count = lax.axis_size(axis)
    leading, last = (max(0, -steps), min(count, count - steps))
    return lax.ppermute(value, axis, [(source, source + steps) for source in range(leading, last)])


def carried_in(value, axis, join, neutral):
    count, mine = (lax.axis_size(axis), lax.axis_index(axis))
    pieces = jax.tree.map(lambda part: lax.all_gather(part, axis), value)
    total = jax.tree.map(
        lambda part, zero: jnp.full_like(part, 0) + jnp.asarray(zero, part.dtype), value, neutral
    )

    def step(position, total):
        longer = join(total, jax.tree.map(lambda part: part[position], pieces))
        return jax.tree.map(lambda new, old: jnp.where(position < mine, new, old), longer, total)

    return lax.fori_loop(0, count - 1, step, total)


def conv_branch(conv_value, conv_gate, conv_taps, conv_bias, channel_gain, channel_shift):
    gated_conv = (
        conv_value.astype(jnp.float32) * jax.nn.sigmoid(conv_gate.astype(jnp.float32))
    ).astype(jnp.bfloat16)
    positions = gated_conv.shape[1]
    reach_rows = conv_taps.shape[0] - 1
    edge_rows = from_behind(gated_conv[:, positions - reach_rows :, :], "sp", 1)
    extended = jnp.concatenate([edge_rows, gated_conv], axis=1)
    filtered = (
        lax.conv_general_dilated(
            extended,
            conv_taps[:, None, :],
            window_strides=(1,),
            padding=[(0, 0)],
            dimension_numbers=("NWC", "WIO", "NWC"),
            feature_group_count=gated_conv.shape[2],
            preferred_element_type=jnp.float32,
        )
        + conv_bias
    )
    row_sums, row_squares = lax.psum(
        (jnp.sum(filtered, axis=-1), jnp.sum(filtered * filtered, axis=-1)), "tp"
    )
    row_mean = (row_sums / D_CONV)[..., None]
    row_var = (row_squares / D_CONV)[..., None] - row_mean * row_mean
    scaled = (filtered - row_mean) * lax.rsqrt(row_var + EPS) * channel_gain + channel_shift
    return jax.nn.silu(scaled).astype(jnp.bfloat16)


def combine_states(earlier, later):
    return (earlier[0] * later[0], later[0][..., None] * earlier[1] + later[1])


def rec_begin(queries, forget_raw, inputs, memory_rate, seq_total):
    seq_count, positions, rec_local = queries.shape
    head_shape = (seq_count, positions, rec_local // HEAD, HEAD)
    rate_rows = (memory_rate / seq_total).reshape(head_shape[2:])
    in_gate = rate_rows * jax.nn.sigmoid(-forget_raw.astype(jnp.float32)).reshape(head_shape)
    cumulative = jnp.cumsum(jnp.log1p(-in_gate), axis=1)
    final_sum = cumulative[:, -1]
    grown = (queries.astype(jnp.float32).reshape(head_shape) * jnp.exp(cumulative)).astype(
        jnp.bfloat16
    )
    shrunk = (in_gate * jnp.exp(-cumulative)).astype(jnp.bfloat16)
    weighted = (in_gate * jnp.exp(final_sum[:, None] - cumulative)).astype(jnp.bfloat16)
    value_rows = inputs.reshape(head_shape)
    causal = jnp.tril(jnp.ones((positions, positions), dtype=bool))
    scores = jnp.einsum("sthk,suhk->shtu", grown, shrunk, preferred_element_type=jnp.float32)
    scores = jnp.where(causal, scores, 0.0).astype(jnp.bfloat16)
    local_out = jnp.einsum(
        "shtu,suhv->sthv", scores, value_rows, preferred_element_type=jnp.float32
    )
    block_decay = jnp.exp(final_sum)
    block_state = jnp.einsum(
        "suhk,suhv->shkv", weighted, value_rows, preferred_element_type=jnp.float32
    )
    identity = (jnp.ones_like(block_decay), jnp.zeros_like(block_state))
    carried = carried_in((block_decay, block_state), "sp", combine_states, identity)
    return (grown, local_out, carried[1])


def rec_finish(grown, local_out, carried_state, out_gate, head_gain):
    carried_low = carried_state.astype(jnp.bfloat16)
    rec_raw = local_out + jnp.einsum(
        "sthk,shkv->sthv", grown, carried_low, preferred_element_type=jnp.float32
    )
    rec_norm = (
        rec_raw
        * lax.rsqrt(jnp.mean(rec_raw * rec_raw, axis=-1, keepdims=True) + EPS)
        * head_gain.reshape(rec_raw.shape[2:])
    )
    return (rec_norm.reshape(out_gate.shape) * jax.nn.silu(out_gate.astype(jnp.float32))).astype(
        jnp.bfloat16
    )


def local(
    frames,
    norm_gain,
    conv_value_w,
    conv_gate_w,
    conv_taps,
    conv_bias,
    channel_gain,
    channel_shift,
    query_w,
    forget_w,
    input_w,
    gate_w,
    memory_rate,
    head_gain,
    conv_out_w,
    rec_out_w,
):
    values = frames.astype(jnp.float32)
    normed = (
        values * lax.rsqrt(jnp.mean(values * values, axis=-1, keepdims=True) + EPS) * norm_gain
    ).astype(jnp.bfloat16)
    conv_local = conv_value_w.shape[1]
    rec_local = query_w.shape[1]
    joined_weight = jnp.concatenate(
        [conv_value_w, conv_gate_w, query_w, forget_w, input_w, gate_w], axis=1
    )
    product = jnp.einsum(
        "spd,dc->spc",
        lax.all_gather(normed, "tp", axis=0, tiled=True),
        joined_weight,
        preferred_element_type=jnp.float32,
    )
    projected = product.astype(jnp.bfloat16)
    split_points = [
        conv_local,
        2 * conv_local,
        2 * conv_local + rec_local,
        2 * conv_local + 2 * rec_local,
        2 * conv_local + 3 * rec_local,
    ]
    conv_value, conv_gate, queries, forget_raw, inputs, out_gate = jnp.split(
        projected, split_points, axis=-1
    )
    seq_total = frames.shape[1] * lax.axis_size("sp")
    conv_out = conv_branch(conv_value, conv_gate, conv_taps, conv_bias, channel_gain, channel_shift)
    grown, local_out, carried_state = rec_begin(queries, forget_raw, inputs, memory_rate, seq_total)
    rec_out = rec_finish(grown, local_out, carried_state, out_gate, head_gain)
    branches = jnp.concatenate([conv_out, rec_out], axis=-1)
    out_weight = jnp.concatenate([conv_out_w, rec_out_w], axis=0)
    full_rows = lax.all_to_all(branches, "tp", split_axis=0, concat_axis=2, tiled=True)
    full_weight = lax.all_gather(out_weight, "tp", axis=0, tiled=True)
    mixed = jnp.einsum("spc,cd->spd", full_rows, full_weight, preferred_element_type=jnp.float32)
    return mixed.astype(jnp.bfloat16)


def solution(mesh):
    placed = (
        P("tp", "sp", None),
        P(),
        P(None, "tp"),
        P(None, "tp"),
        P(None, "tp"),
        P("tp"),
        P("tp"),
        P("tp"),
        P(None, "tp"),
        P(None, "tp"),
        P(None, "tp"),
        P(None, "tp"),
        P("tp"),
        P("tp"),
        P("tp", None),
        P("tp", None),
    )
    return jax.shard_map(
        local, mesh=mesh, in_specs=placed, out_specs=P("tp", "sp", None), check_vma=False
    )
```

profile of v0, /device:TPU:0, one launch (start us, length us, event | category | flops | bytes accessed | tf_op | source)
XLA Modules:
  0.0 153.3 jit_solution(11214979826300616397)
XLA Ops:
  6.5 0.0 copy-start
  6.5 0.0 all-gather.6.cloned.1.call-start
  6.6 1.2 fusion.6
  7.8 1.8 %fusion.8 = bf16[1,128,1024]{2,1,0:T(8,128)(2,1)} fusion(bf16[1,128,1024]{2,1,0:T(8,128)(2,1)} %param.18, f32[1024]{0:T(1024)} %param.19, f32[128]{0:T(128)S(1)} %add_rsqrt_fusion.2), kind=kLoop, calls=%fused_computation.19 | loop fusion | flops 524288 | bytes 528896 | tf_op jit(solution)/shard_map/convert_element_type | solution.py:130
  9.6 0.0 all-gather.6.cloned.1.call-update
  9.6 0.0 copy-start.9
  9.6 0.0 all-gather.10.cloned.1.call-start
  9.7 1.7 %constant_dynamic-update-slice_fusion.5 = bf16[1024,1280]{1,0:T(8,128)(2,1)} fusion(bf16[1024,128]{1,0:T(8,128)(2,1)} %param.20), kind=kLoop, calls=%fused_computation.66 | loop fusion | bytes 524288
  11.4 1.7 %constant_dynamic-update-slice_fusion.4 = bf16[1024,1280]{1,0:T(8,128)(2,1)} fusion(bf16[1024,1280]{1,0:T(8,128)(2,1)} %constant_dynamic-update-slice_fusion.5, bf16[1024,128]{1,0:T(8,128)(2,1)} %param.21), kind=kLoop, calls=%fused_computation.65 | loop fusion | bytes 524288
  13.1 1.9 %constant_dynamic-update-slice_fusion.3 = bf16[1024,1280]{1,0:T(8,128)(2,1)} fusion(bf16[1024,1280]{1,0:T(8,128)(2,1)} %constant_dynamic-update-slice_fusion.4, bf16[1024,256]{1,0:T(8,128)(2,1)} %param.26), kind=kLoop, calls=%fused_computation.64 | loop fusion | bytes 1048576
  15.0 0.0 copy-done.3
  15.0 0.9 constant_dynamic-update-slice_fusion.2
  15.9 0.0 copy-done.4
  15.9 0.9 constant_dynamic-update-slice_fusion.1
  16.8 0.0 copy-done.5
  16.8 0.9 constant_dynamic-update-slice_fusion
  17.7 0.0 copy-done.9
  17.7 11.5 %all-gather.6.cloned.1.call-done = bf16[4,128,1024]{2,1,0:T(8,128)(2,1)} async-done(((bf16[1,128,1024]{2,1,0:T(8,128)(2,1)}), bf16[4,128,1024]{2,1,0:T(8,128)(2,1)}) %all-gather.6.cloned.1.call-update) | async-done | bytes 1048592 | tf_op jit(solution)/shard_map/all_gather | solution.py:138
  29.2 3.6 %convolution_convert_fusion = bf16[4,128,1280]{2,1,0:T(8,128)(2,1)S(1)} fusion(bf16[4,128,1024]{2,1,0:T(8,128)(2,1)} %all-gather.6.cloned.1.call-done, bf16[1024,1280]{1,0:T(8,128)(2,1)} %constant_dynamic-update-slice_fusion), kind=kOutput, calls=%fused_computation.3 | convolution fusion | flops 1342832640 | bytes 4980736 | tf_op jit(solution)/shard_map/spd,dc->spc/dot_general | solution.py:136
  32.8 0.0 copy-start.1
  32.8 0.1 add_divide_fusion
  32.9 1.0 copy-done.1
  33.9 0.1 slice_convert_fusion
  34.0 0.3 reshape.71
  34.3 0.8 fusion.13
  35.1 0.0 copy-start.2
  35.1 0.0 copy-start.6
  35.2 0.3 reshape.75
  35.5 1.0 multiply_convert_fusion
  36.4 1.1 fusion.19
  37.5 0.0 all-gather.10.cloned.1.call-update
  37.5 0.0 all-gather.8.cloned.1.call-start
  37.6 1.0 pad_maximum_fusion
  38.6 0.0 all-gather.8.cloned.1.call-update
  38.7 1.1 multiply_convert_fusion.4
  39.8 3.4 %collective-permute-start = (bf16[4,30,128]{2,1,0:T(8,128)(2,1)S(1)}, bf16[4,30,128]{2,1,0:T(8,128)(2,1)S(1)}, u32[]{:S(2)}, u32[]{:S(2)}) collective-permute-start(bf16[4,30,128]{2,1,0:T(8,128)(2,1)S(1)} %slice.8), channel_id=1, source_target_pairs={{0,4},{4,8},{8,12},{12,16},{16,20},{20,24},{24,28},{1,5},{5,9},{9,... | collective-permute-start | bytes 92168 | tf_op jit(solution)/shard_map/ppermute | solution.py:16
  43.2 0.5 fusion.5
  43.6 0.0 copy-start.7
  43.7 0.0 copy-start.10
  43.7 0.0 copy-start.11
  43.7 31.6 %all-gather = f32[32,1,2,128]{3,2,1,0:T(2,128)S(1)} all-gather(f32[4,1,2,128]{3,2,1,0:T(2,128)S(1)} %get-tuple-element.138), channel_id=2, replica_groups=mesh['sp'=8,'tp'=4] {'sp'}, dimensions={0}, use_global_device_ids=true | all-gather | bytes 36864 | tf_op jit(solution)/shard_map/all_gather | solution.py:21
  75.3 0.0 collective-permute-done
  75.3 0.7 fusion.34
  76.0 0.2 fusion.33
  76.3 6.1 %all-reduce = (f32[4,128]{1,0:T(4,128)S(1)}, f32[4,128]{1,0:T(4,128)S(1)}) all-reduce(f32[4,128]{1,0:T(4,128)S(1)} %get-tuple-element.119, f32[4,128]{1,0:T(4,128)S(1)} %get-tuple-element.118), channel_id=1, replica_groups=mesh['sp'=8,'tp'=4] {'tp'}, use_global_device_ids=true, to_apply=%region_4.0 | all-reduce | flops 1024 | bytes 8192 | tf_op jit(solution)/shard_map/psum | solution.py:53
  82.3 0.2 multiply_convert_fusion.3
  82.6 28.1 %all-gather.10.cloned.1.call-done = f32[32,2,128,128]{3,2,1,0:T(8,128)} async-done(((f32[4,2,128,128]{3,2,1,0:T(8,128)}), f32[32,2,128,128]{3,2,1,0:T(8,128)}) %all-gather.10.cloned.1.call-update) | async-done | bytes 4194320 | tf_op jit(solution)/shard_map/all_gather | solution.py:21
  110.7 10.1 %while.14 = (s32[]{:T(128)}, f32[4,2,128,128]{3,2,1,0:T(8,128)S(1)}, s32[]{:T(128)}, f32[8,4,2,128]{3,2,1,0:T(2,128)S(1)}, f32[8,4,2,128,128]{4,3,2,1,0:T(8,128)}, /*index=5*/s32[]{:T(128)}, s32[]{:T(128)}) while((s32[]{:T(128)}, f32[4,2,128,128]{3,2,1,0:T(8,128)S(1)}, s32[]{:T(128)}, f32[8,4,2,128]{3,2,1,0:T(2,128)S(1)}, ...), condition=%wide.region_7.8_spmd.clone, body=%wide.region_6.7_spmd.clone.sunk | while | flops 524292 | bytes 1585257 | solution.py:30
  110.7 1.4 fusion.42
  112.2 1.4 fusion.42
  113.6 1.4 fusion.42
  115.0 1.4 fusion.42
  116.4 1.4 fusion.42
  117.9 1.4 fusion.42
  119.4 1.4 fusion.42
  120.8 0.4 multiply_reduce_fusion
  121.2 0.1 multiply_multiply_fusion
  121.3 0.2 copy.49
  121.5 1.1 fusion.16
  122.6 0.1 pad_maximum_fusion.1
  122.7 14.6 %all_to_all.15 = bf16[4,128,384]{2,1,0:T(8,128)(2,1)S(1)} all-to-all(bf16[4,128,384]{2,1,0:T(8,128)(2,1)S(1)} %pad_maximum_fusion.1), channel_id=1, replica_groups=mesh['sp'=8,'tp'=4] {'tp'}, dimensions={0} | all-to-all | bytes 786432 | tf_op jit(solution)/shard_map/all_to_all | solution.py:159
  137.3 0.2 copy.47
  137.5 6.0 %all-gather.8.cloned.1.call-done = bf16[1536,1024]{1,0:T(8,128)(2,1)} async-done(((bf16[384,1024]{1,0:T(8,128)(2,1)}), bf16[1536,1024]{1,0:T(8,128)(2,1)}) %all-gather.8.cloned.1.call-update) | async-done | bytes 3145744 | tf_op jit(solution)/shard_map/all_gather | solution.py:160
  143.6 3.2 %fusion.4 = bf16[1,128,1024]{2,1,0:T(8,128)(2,1)} fusion(bf16[128,1536]{0,1:T(8,128)(2,1)S(1)} %bitcast.43, bf16[1536,1024]{1,0:T(8,128)(2,1)} %all-gather.8.cloned.1.call-done), kind=kOutput, calls=%fused_computation.10 | convolution fusion | flops 402784256 | bytes 3801088 | tf_op jit(solution)/shard_map/spc,cd->spd/dot_general | solution.py:161
  (27 shorter events, 0.2 us)
Async XLA Ops:
  6.5 68.8 %copy-start = (bf16[31,128]{1,0:T(8,128)(2,1)S(1)}, bf16[31,128]{1,0:T(8,128)(2,1)}, u32[]{:S(2)}) copy-start(bf16[31,128]{1,0:T(8,128)(2,1)} %param.22) | copy-start | bytes 23812
  6.5 8.5 %copy-start.3 = (bf16[1024,256]{1,0:T(8,128)(2,1)S(1)}, bf16[1024,256]{1,0:T(8,128)(2,1)}, u32[]{:S(2)}) copy-start(bf16[1024,256]{1,0:T(8,128)(2,1)} %param.27) | copy-start | bytes 1572868
  6.5 9.3 %copy-start.4 = (bf16[1024,256]{1,0:T(8,128)(2,1)S(1)}, bf16[1024,256]{1,0:T(8,128)(2,1)}, u32[]{:S(2)}) copy-start(bf16[1024,256]{1,0:T(8,128)(2,1)} %param.28) | copy-start | bytes 1572868
  6.5 10.2 %copy-start.5 = (bf16[1024,256]{1,0:T(8,128)(2,1)S(1)}, bf16[1024,256]{1,0:T(8,128)(2,1)}, u32[]{:S(2)}) copy-start(bf16[1024,256]{1,0:T(8,128)(2,1)} %param.29) | copy-start | bytes 1572868
  6.5 22.6 %all-gather.6.cloned.1.call-start = ((), (), s32[]{:S(2)}) async-start(), calls=%async_computation.1 | async-start | bytes 1310720 | tf_op jit(solution)/shard_map/all_gather | solution.py:138
  9.6 8.1 %copy-start.9 = (f32[256]{0:T(256)S(1)}, f32[256]{0:T(256)}, u32[]{:S(2)}) copy-start(f32[256]{0:T(256)} %param.30) | copy-start | bytes 3076
  9.6 101.1 %all-gather.10.cloned.1.call-start = ((), (), s32[]{:S(2)}) async-start(), calls=%async_computation.3 | async-start | bytes 4718592 | tf_op jit(solution)/shard_map/all_gather | solution.py:21
  32.8 1.2 copy-start.1
  35.1 2.4 %copy-start.2 = (bf16[256,1024]{1,0:T(8,128)(2,1)S(1)}, bf16[256,1024]{1,0:T(8,128)(2,1)}, u32[]{:S(2)}) copy-start(bf16[256,1024]{1,0:T(8,128)(2,1)} %param.33) | copy-start | bytes 1572868
  35.1 2.4 %copy-start.6 = (bf16[128,1024]{1,0:T(8,128)(2,1)S(1)}, bf16[128,1024]{1,0:T(8,128)(2,1)}, u32[]{:S(2)}) copy-start(bf16[128,1024]{1,0:T(8,128)(2,1)} %param.32) | copy-start | bytes 786436
  37.5 106.0 %all-gather.8.cloned.1.call-start = ((), (), s32[]{:S(2)}) async-start(), calls=%async_computation.2 | async-start | bytes 3932160 | tf_op jit(solution)/shard_map/all_gather | solution.py:160
  39.8 35.5 %collective-permute-start = (bf16[4,30,128]{2,1,0:T(8,128)(2,1)S(1)}, bf16[4,30,128]{2,1,0:T(8,128)(2,1)S(1)}, u32[]{:S(2)}, u32[]{:S(2)}) collective-permute-start(bf16[4,30,128]{2,1,0:T(8,128)(2,1)S(1)} %slice.8), channel_id=1, source_target_pairs={{0,4},{4,8},{8,12},{12,16},{16,20},{20,24},{24,28},{1,5},{5,9},{9,... | collective-permute-start | bytes 92168 | tf_op jit(solution)/shard_map/ppermute | solution.py:16
  43.6 32.4 %copy-start.7 = (f32[128]{0:T(128)S(1)}, f32[128]{0:T(128)}, u32[]{:S(2)}) copy-start(f32[128]{0:T(128)} %param.23) | copy-start | bytes 1540
  43.7 38.7 %copy-start.10 = (f32[128]{0:T(128)S(1)}, f32[128]{0:T(128)}, u32[]{:S(2)}) copy-start(f32[128]{0:T(128)} %param.25) | copy-start | bytes 1540
  43.7 38.7 %copy-start.11 = (f32[128]{0:T(128)S(1)}, f32[128]{0:T(128)}, u32[]{:S(2)}) copy-start(f32[128]{0:T(128)} %param.24) | copy-start | bytes 1540
  110.7 10.5 %copy-start.8 = (f32[256]{0:T(256)S(1)}, f32[256]{0:T(256)}, u32[]{:S(2)}) copy-start(f32[256]{0:T(256)} %param.31) | copy-start | bytes 3076
Sparse Core Ops, SparseCore 0:
  9.7 19.4 all-gather.5
  37.6 73.0 all-gather.9
  112.3 31.2 all-gather.7
where the time goes:
time: 154 us; the launch traced here: 153 us
  blocking collectives  52.3 us (34%)
  waiting for transfers between devices  45.7 us (30%)
  other arithmetic  18.7 us (12%)
  between operations  13.4 us (9%)
  local copies, waits for them, and re-layouts  10.1 us (7%)
  matrix products  9.42 us (6%)
  starting transfers between devices  3.5 us (2%)
    all_gather x1, blocking collectives, carried_in(): pieces = jax.tree.map(lambda part: lax.all_gather(part, axis), value)  31.6 us
    all_gather x1, waiting for transfers between devices, carried_in(): pieces = jax.tree.map(lambda part: lax.all_gather(part, axis), value)  28.1 us
    all_to_all x1, blocking collectives, local(): lax.all_to_all(branches, 'tp', split_axis=0, concat_axis=2, tiled=True)  14.6 us
    all_gather x1, waiting for transfers between devices, local(): lax.all_gather(normed, 'tp', axis=0, tiled=True)  11.5 us
    select_n x7, other arithmetic, step(): jnp.where(position < mine, new, old)  9.82 us
    unnamed x29, local copies, waits for them, and re-layouts  8.15 us
    psum x1, blocking collectives, conv_branch(): lax.psum((jnp.sum(filtered, axis=-1), jnp.sum(filtered * filtered, axis=-...  6.07 us
    all_gather x1, waiting for transfers between devices, local(): full_weight = lax.all_gather(out_weight, 'tp', axis=0, tiled=True)  6.03 us
  transfers between devices with their start and end apart: 4, of which 3 were waited for; matrix products, arithmetic and copies ran while one was open for 15% of the time, Pallas kernels for 0%

commit v1 on v0

v1 whole, which is shorter than its diff:
```python
import functools

import jax
import jax.numpy as jnp
from jax import lax
from jax.experimental import pallas as pl
from jax.experimental.pallas import tpu as pltpu
from jax.sharding import PartitionSpec as P

HEAD = 128
LANES = 128
EDGE = 32
EPS = 1e-06
MESH = pl.DeviceIdType.MESH
F32 = jnp.float32
BF16 = jnp.bfloat16


def flip(index, mask):
    out, bit = index, 1
    while bit <= mask:
        if mask & bit:
            out = out + bit - 2 * bit * ((index // bit) % 2)
        bit *= 2
    return out


def mm(a, b, dims):
    return lax.dot_general(a, b, (dims, ((), ())), preferred_element_type=F32)


def kernel(
    cfg,
    frames, norm_gain, cvw, cgw, taps, conv_bias, channel_gain, channel_shift,
    qw, fw, iw, gw, rate, head_gain, cow, row,
    out,
    gath, wbuf, ow, norm_v, taps_v, cb_v, cg_v, cs_v, rate_v, hg_v,
    gated, edges, ext, filt, stat, stat_in, conv_send, conv_in, rec_send, rec_in,
    grown_s, shrunk_s, value_s, gate_s, local_s, state, state_in, decay, decay_in, carry_out, carry_in, acc,
    loc_sem, fr_send, fr_recv, ow_send, ow_recv, ed_send, ed_recv, stt_send, stt_recv, dc_send, dc_recv,
    ca_send, ca_recv, sm_send, sm_recv, cv_send, cv_recv, rc_send, rc_recv,
):
    n_tp, n_sp, spt, d_conv, seq_total = cfg
    positions, depth = frames.shape[1], frames.shape[2]
    seqs = n_tp * spt
    conv_n, rec_n = cvw.shape[1], qw.shape[1]
    heads = rec_n // HEAD
    chunk = carry_out.shape[1]
    tp, sp = lax.axis_index("tp"), lax.axis_index("sp")

    barrier = pltpu.get_barrier_semaphore()
    for k in range(1, n_tp):
        pl.semaphore_signal(barrier, inc=1, device_id={"tp": flip(tp, k)}, device_id_type=MESH)
    for d in range(1, n_sp):
        pl.semaphore_signal(barrier, inc=1, device_id={"sp": (sp + d) % n_sp}, device_id_type=MESH)

    offsets = [0, conv_n, 2 * conv_n, 2 * conv_n + rec_n, 2 * conv_n + 2 * rec_n, 2 * conv_n + 3 * rec_n]
    copies = [pltpu.make_async_copy(frames, gath.at[0], loc_sem.at[0])]
    copies.append(pltpu.make_async_copy(norm_gain, norm_v, loc_sem.at[1]))
    for n, (ref, at) in enumerate(zip((cvw, cgw, qw, fw, iw, gw), offsets)):
        copies.append(
            pltpu.make_async_copy(ref, wbuf.at[:, pl.ds(at, ref.shape[1])], loc_sem.at[2 + n])
        )
    small = ((taps, taps_v), (conv_bias, cb_v), (channel_gain, cg_v), (channel_shift, cs_v), (rate, rate_v), (head_gain, hg_v))
    for n, (ref, to) in enumerate(small):
        copies.append(pltpu.make_async_copy(ref, to, loc_sem.at[8 + n]))
    copies.append(pltpu.make_async_copy(cow, ow.at[0, pl.ds(0, conv_n)], loc_sem.at[14]))
    copies.append(pltpu.make_async_copy(row, ow.at[0, pl.ds(conv_n, rec_n)], loc_sem.at[15]))
    for copy in copies:
        copy.start()

    def remote(src, dst, send, recv, **device):
        return pltpu.make_async_remote_copy(
            src_ref=src, dst_ref=dst, send_sem=send, recv_sem=recv, device_id=device, device_id_type=MESH
        )

    direct = [k for k in range(1, n_tp) if k % 2 == 0] + [1]
    fr = [None] * n_tp
    for k in range(1, n_tp):
        if k in direct:
            fr[k] = remote(frames, gath.at[k], fr_send.at[k], fr_recv.at[k], tp=flip(tp, k))
        else:
            fr[k] = remote(gath.at[k - 1], gath.at[k], fr_send.at[k], fr_recv.at[k], tp=flip(tp, 1))
    wt = [None] * n_tp
    for k in range(1, n_tp):
        source, to = (0, k) if k in direct else (k - 1, 1)
        wt[k] = remote(ow.at[source], ow.at[k], ow_send.at[k], ow_recv.at[k], tp=flip(tp, to))

    pl.semaphore_wait(barrier, n_tp - 1 + n_sp - 1)
    for k in direct:
        fr[k].start()
    for copy in copies:
        copy.wait()

    t_row = lax.broadcasted_iota(jnp.int32, (positions, positions), 0)
    t_col = lax.broadcasted_iota(jnp.int32, (positions, positions), 1)
    causal = t_col <= t_row
    lower = jnp.where(causal, 1.0, 0.0).astype(BF16)
    lower3 = jnp.concatenate([lower, lower, lower], axis=1)
    rate_row = rate_v[...] / seq_total

    sent_states = []

    def state_copies(p):
        pair = p * chunk // HEAD
        return (
            remote(state.at[pl.ds(p * chunk, chunk)], state_in.at[sp], stt_send.at[p], stt_recv.at[sp], sp=p),
            remote(decay.at[pair], decay_in.at[sp], dc_send.at[p], dc_recv.at[sp], sp=p),
        )

    def edge_copy(q):
        return remote(
            gated.at[q, pl.ds(positions - EDGE, EDGE)], edges.at[q], ed_send.at[q], ed_recv.at[q], sp=(sp + 1) % n_sp
        )

    for k in range(n_tp):
        if k > 0:
            fr[k].wait_recv()
            if k % 2 == 0:
                fr[k + 1].start()
        if k == min(2, n_tp - 1):
            for j in direct:
                wt[j].start()
        for i in range(spt):
            q = k * spt + i
            x = gath[k, i].astype(F32)
            mean = jnp.mean(x * x, axis=-1, keepdims=True)
            normed = (x * lax.rsqrt(mean + EPS) * norm_v[...]).astype(BF16)

            def project(at, width):
                return mm(normed, wbuf[:, at : at + width], ((1,), (0,))).astype(BF16)

            conv_both = project(0, 2 * conv_n).astype(F32)
            gated_q = (conv_both[:, :conv_n] * jax.nn.sigmoid(conv_both[:, conv_n:])).astype(BF16)
            gated[q] = gated_q
            ext[q, EDGE : EDGE + positions] = gated_q.astype(F32)
            edge_copy(q).start()

            forget_raw = project(offsets[3], rec_n).astype(F32)
            in_gate = rate_row * jax.nn.sigmoid(-forget_raw)
            log_forget = jnp.log1p(-in_gate)
            hi = log_forget.astype(BF16)
            rest = log_forget - hi.astype(F32)
            mid = rest.astype(BF16)
            low = (rest - mid.astype(F32)).astype(BF16)
            cumulative = mm(lower3, jnp.concatenate([hi, mid, low], axis=0), ((1,), (0,)))
            last = cumulative[positions - 1 : positions, :]
            weighted = (in_gate * jnp.exp(last - cumulative)).astype(BF16)
            value = project(offsets[4], rec_n)
            value_s[q] = value
            last_decay = jnp.exp(last)
            for h in range(heads):
                pair = q * heads + h
                lanes = slice(h * HEAD, (h + 1) * HEAD)
                state[pair * HEAD : (pair + 1) * HEAD] = mm(value[:, lanes], weighted[:, lanes], ((0,), (0,)))
                decay[pair] = jnp.broadcast_to(last_decay[:, lanes], (8, HEAD))
                for p in range(pair * HEAD // chunk, (pair + 1) * HEAD // chunk):

                    @pl.when(jnp.logical_and(sp != p, sp < n_sp - 1))
                    def _():
                        for copy in state_copies(p):
                            copy.start()

            shrunk_s[q] = (in_gate * jnp.exp(-cumulative)).astype(BF16)
            queries = project(offsets[2], rec_n).astype(F32)
            grown_s[q] = (queries * jnp.exp(cumulative)).astype(BF16)
            gate_s[q] = project(offsets[5], rec_n)

    reach = taps.shape[0] - 1
    for q in range(seqs):
        edge_copy(q).wait_recv()
        ext[q, 0:EDGE] = jnp.where(sp > 0, edges[q].astype(F32), 0.0)
        total = jnp.broadcast_to(cb_v[...], (positions, conv_n))
        tap_rows = taps_v[...].astype(F32)
        for j in range(reach + 1):
            start = EDGE - reach + j
            total = total + tap_rows[j : j + 1, :] * ext[q, start : start + positions, :]
        filt[q] = total
        lane = lax.broadcasted_iota(jnp.int32, (positions, LANES), 1)
        sums = jnp.sum(total, axis=-1, keepdims=True)
        squares = jnp.sum(total * total, axis=-1, keepdims=True)
        table = jnp.where(lane == 0, sums, jnp.where(lane == 1, squares, 0.0))
        stat[q] = jnp.transpose(table)[0:8, :]

    def stat_copy(k):
        return remote(stat, stat_in.at[k], sm_send.at[k], sm_recv.at[k], tp=flip(tp, k))

    for k in range(1, n_tp):
        stat_copy(k).start()

    own = pl.multiple_of(sp * chunk, chunk)
    state_in[sp] = state[pl.ds(own, chunk), :]
    decay_in[sp] = decay[sp * chunk // HEAD]

    def carry_copy(j):
        return remote(carry_out.at[j], carry_in.at[pl.ds(own, chunk)], ca_send.at[j], ca_recv.at[sp], sp=j)

    def from_source(j):
        return (
            remote(state.at[pl.ds(0, chunk)], state_in.at[j], stt_send.at[j], stt_recv.at[j], sp=j),
            remote(decay.at[0], decay_in.at[j], dc_send.at[j], dc_recv.at[j], sp=j),
        )

    carried = jnp.zeros((chunk, HEAD), F32)
    for j in range(n_sp):
        carry_out[j] = carried.astype(BF16)
        if j > 0:

            @pl.when(sp != j)
            def _():
                carry_copy(j).start()

        if j < n_sp - 1:

            @pl.when(sp != j)
            def _():
                for copy in from_source(j):
                    copy.wait_recv()

            carried = decay_in[j, 0:1, :] * carried + state_in[j]
    carry_in[pl.ds(own, chunk), :] = carry_out[sp]

    for q in range(seqs):
        for h in range(heads):
            lanes = slice(h * HEAD, (h + 1) * HEAD)
            scores = mm(grown_s[q, :, lanes], shrunk_s[q, :, lanes], ((1,), (1,)))
            scores = jnp.where(causal, scores, 0.0).astype(BF16)
            local_s[q, :, lanes] = mm(scores, value_s[q, :, lanes], ((1,), (0,)))

    for k in range(1, n_tp):
        stat_copy(k).wait_recv()

    def conv_copy(k):
        return remote(conv_send.at[k], conv_in.at[k], cv_send.at[k], cv_recv.at[k], tp=flip(tp, k))

    def rec_copy(k):
        return remote(rec_send.at[k], rec_in.at[k], rc_send.at[k], rc_recv.at[k], tp=flip(tp, k))

    order = list(range(n_tp - 1, -1, -1))
    for k in order:
        for i in range(spt):
            q = k * spt + i
            both = stat[q]
            for d in range(1, n_tp):
                both = both + stat_in[d, (k ^ d) * spt + i]
            both = both / d_conv
            table = jnp.concatenate([both, jnp.zeros((LANES - 8, positions), F32)], axis=0)
            table = jnp.transpose(table)
            row_mean = table[:, 0:1]
            row_var = table[:, 1:2] - row_mean * row_mean
            scaled = (filt[q] - row_mean) * lax.rsqrt(row_var + EPS) * cg_v[...] + cs_v[...]
            result = (scaled * jax.nn.sigmoid(scaled)).astype(BF16)
            rows = slice(i * positions, (i + 1) * positions)
            if k == 0:
                conv_in[0, rows] = result
            else:
                conv_send[k, rows] = result
        if k > 0:
            conv_copy(k).start()

    for j in range(n_sp):

        @pl.when(jnp.logical_and(sp != j, sp > 0))
        def _():
            remote(
                carry_out.at[0], carry_in.at[pl.ds(j * chunk, chunk)], ca_send.at[j], ca_recv.at[j], sp=j
            ).wait_recv()

    @pl.when(sp == 0)
    def _():
        carry_in[...] = jnp.zeros_like(carry_in)

    for k in order:
        for i in range(spt):
            q = k * spt + i
            rows = slice(i * positions, (i + 1) * positions)
            for h in range(heads):
                pair = q * heads + h
                lanes = slice(h * HEAD, (h + 1) * HEAD)
                rec_raw = local_s[q, :, lanes] + mm(
                    grown_s[q, :, lanes], carry_in[pair * HEAD : (pair + 1) * HEAD, :], ((1,), (1,))
                )
                mean = jnp.mean(rec_raw * rec_raw, axis=-1, keepdims=True)
                rec_norm = rec_raw * lax.rsqrt(mean + EPS) * hg_v[:, lanes]
                gate = gate_s[q, :, lanes].astype(F32)
                result = (rec_norm * (gate * jax.nn.sigmoid(gate))).astype(BF16)
                if k == 0:
                    rec_in[0, rows, lanes] = result
                else:
                    rec_send[k, rows, lanes] = result
        if k > 0:
            rec_copy(k).start()

    for k in range(2, n_tp, 2):
        wt[k].wait_recv()
        wt[k + 1].start()
    if n_tp > 1:
        wt[1].wait_recv()
    for n, k in enumerate(range(n_tp)):
        if k > 0:
            if k % 2 == 1 and k > 1:
                wt[k].wait_recv()
            conv_copy(k).wait_recv()
            rec_copy(k).wait_recv()
        part = mm(conv_in[k], ow[k, 0:conv_n, :], ((1,), (0,))) + mm(
            rec_in[k], ow[k, conv_n : conv_n + rec_n, :], ((1,), (0,))
        )
        if k == 0:
            acc[...] = part
        elif k < n_tp - 1:
            acc[...] += part
        else:
            out[...] = (acc[...] + part).astype(BF16).reshape(out.shape)

    for k in range(1, n_tp):
        fr[k].wait_send()
        wt[k].wait_send()
        stat_copy(k).wait_send()
        conv_copy(k).wait_send()
        rec_copy(k).wait_send()
    for q in range(seqs):
        edge_copy(q).wait_send()
    for p in range(n_sp):

        @pl.when(jnp.logical_and(sp != p, sp < n_sp - 1))
        def _():
            for copy in state_copies(p):
                copy.wait_send()

        if p > 0:

            @pl.when(sp != p)
            def _():
                carry_copy(p).wait_send()


def wide(array, axis):
    extra = -array.shape[axis] % LANES
    if extra == 0:
        return array
    pads = [(0, 0)] * array.ndim
    pads[axis] = (0, extra)
    return jnp.pad(array, pads)


def local(
    n_tp, n_sp, frames, norm_gain, conv_value_w, conv_gate_w, conv_taps, conv_bias, channel_gain, channel_shift,
    query_w, forget_w, input_w, gate_w, memory_rate, head_gain, conv_out_w, rec_out_w,
):
    d_conv = conv_value_w.shape[1] * n_tp
    spt, positions, depth = frames.shape
    conv_value_w, conv_gate_w, conv_taps = (wide(a, 1) for a in (conv_value_w, conv_gate_w, conv_taps))
    conv_bias, channel_gain, channel_shift, conv_out_w = (
        wide(a, 0) for a in (conv_bias, channel_gain, channel_shift, conv_out_w)
    )
    conv_n, rec_n = conv_value_w.shape[1], query_w.shape[1]
    out_n = rec_out_w.shape[1]
    seqs = n_tp * spt
    heads = rec_n // HEAD
    pairs = seqs * heads
    chunk = pairs * HEAD // n_sp
    width = conv_n * 2 + rec_n * 4
    rows = spt * positions
    vm = pltpu.VMEM
    sem = pltpu.SemaphoreType.DMA
    scratch = [
        vm((n_tp, spt, positions, depth), BF16),
        vm((depth, width), BF16),
        vm((n_tp, conv_n + rec_n, out_n), BF16),
        vm((1, depth), F32),
        vm(conv_taps.shape, BF16),
        vm((1, conv_n), F32),
        vm((1, conv_n), F32),
        vm((1, conv_n), F32),
        vm((1, rec_n), F32),
        vm((1, rec_n), F32),
        vm((seqs, positions, conv_n), BF16),
        vm((seqs, EDGE, conv_n), BF16),
        vm((seqs, EDGE + positions, conv_n), F32),
        vm((seqs, positions, conv_n), F32),
        vm((seqs, 8, positions), F32),
        vm((n_tp, seqs, 8, positions), F32),
        vm((n_tp, rows, conv_n), BF16),
        vm((n_tp, rows, conv_n), BF16),
        vm((n_tp, rows, rec_n), BF16),
        vm((n_tp, rows, rec_n), BF16),
        vm((seqs, positions, rec_n), BF16),
        vm((seqs, positions, rec_n), BF16),
        vm((seqs, positions, rec_n), BF16),
        vm((seqs, positions, rec_n), BF16),
        vm((seqs, positions, rec_n), F32),
        vm((pairs * HEAD, HEAD), F32),
        vm((n_sp, chunk, HEAD), F32),
        vm((pairs, 8, HEAD), F32),
        vm((n_sp, 8, HEAD), F32),
        vm((n_sp, chunk, HEAD), BF16),
        vm((pairs * HEAD, HEAD), BF16),
        vm((rows, out_n), F32),
        sem((16,)),
        sem((n_tp,)), sem((n_tp,)),
        sem((n_tp,)), sem((n_tp,)),
        sem((seqs,)), sem((seqs,)),
        sem((n_sp,)), sem((n_sp,)),
        sem((n_sp,)), sem((n_sp,)),
        sem((n_sp,)), sem((n_sp,)),
        sem((n_tp,)), sem((n_tp,)),
        sem((n_tp,)), sem((n_tp,)),
        sem((n_tp,)), sem((n_tp,)),
    ]
    return pl.pallas_call(
        functools.partial(kernel, (n_tp, n_sp, spt, d_conv, positions * n_sp)),
        out_shape=jax.ShapeDtypeStruct((spt, positions, out_n), BF16),
        in_specs=[pl.BlockSpec(memory_space=pl.ANY)] * 16,
        out_specs=pl.BlockSpec(memory_space=pltpu.VMEM),
        scratch_shapes=scratch,
        compiler_params=pltpu.CompilerParams(
            collective_id=0, has_side_effects=True, vmem_limit_bytes=48 * 1024 * 1024
        ),
    )(
        frames, norm_gain[None], conv_value_w, conv_gate_w, conv_taps, conv_bias[None], channel_gain[None],
        channel_shift[None], query_w, forget_w, input_w, gate_w, memory_rate[None], head_gain[None],
        conv_out_w, rec_out_w,
    )


def solution(mesh):
    placed = (
        P("tp", "sp", None),
        P(),
        P(None, "tp"),
        P(None, "tp"),
        P(None, "tp"),
        P("tp"),
        P("tp"),
        P("tp"),
        P(None, "tp"),
        P(None, "tp"),
        P(None, "tp"),
        P(None, "tp"),
        P("tp"),
        P("tp"),
        P("tp", None),
        P("tp", None),
    )
    return jax.shard_map(
        functools.partial(local, mesh.shape["tp"], mesh.shape["sp"]),
        mesh=mesh, in_specs=placed, out_specs=P("tp", "sp", None), check_vma=False,
    )
```

time: 154 us -> 52.4 us (0.34)
  blocking collectives: 52.3 us -> 0 us
  waiting for transfers between devices: 45.7 us -> 0 us
  Pallas kernels: 0 us -> 40 us
  other arithmetic: 18.7 us -> 0 us
  between operations: 13.4 us -> 0.03 us
  matrix products: 9.42 us -> 0 us
  starting transfers between devices: 3.5 us -> 0 us
  local copies, waits for them, and re-layouts: 10.1 us -> 11.8 us
    all_gather x3 -> x0, waiting for transfers between devices: 45.7 us -> none  [the longest x1 28.1 us: carried_in(): pieces = jax.tree.map(lambda part: lax.all_gather(part, axis), value)]
    pallas_call x0 -> x1, Pallas kernels: none -> 40 us  [local(): pl.pallas_call(functools.partial(kernel, (n_tp, n_sp, spt, d_conv, positi...]
    all_gather x1 -> x0, blocking collectives: 31.6 us -> none  [carried_in(): pieces = jax.tree.map(lambda part: lax.all_gather(part, axis), value)]
    all_to_all x1 -> x0, blocking collectives: 14.6 us -> none  [local(): lax.all_to_all(branches, 'tp', split_axis=0, concat_axis=2, tiled=True)]
    select_n x7 -> x0, other arithmetic: 9.82 us -> none  [step(): jnp.where(position < mine, new, old)]
    dot_general x5 -> x0, matrix products: 8.71 us -> none  [the longest x1 3.58 us: local(): jnp.einsum('spd,dc->spc', lax.all_gather(normed, 'tp', axis=0, tiled=True...]
    psum x1 -> x0, blocking collectives: 6.07 us -> none  [conv_branch(): lax.psum((jnp.sum(filtered, axis=-1), jnp.sum(filtered * filtered, axis=-...]
    convert_element_type x5 -> x0, other arithmetic: 5.14 us -> none  [the longest x1 1.79 us: local(): normed = (values * lax.rsqrt(jnp.mean(values * values, axis=-1, keepdims=...]
  transfers between devices with their start and end apart: 4 -> 0, of which waited for: 3 -> 0; matrix products, arithmetic and copies ran while one was open for 15% -> 0% of each run, Pallas kernels for 0% -> 0%
where the time goes in v1:
time: 52.4 us; the launch traced here: 51.8 us
  Pallas kernels  40 us (76%)
  local copies, waits for them, and re-layouts  11.8 us (23%)
    pallas_call x1, Pallas kernels, local(): pl.pallas_call(functools.partial(kernel, (n_tp, n_sp, spt, d_conv, positi...  40 us
    unnamed x33, local copies, waits for them, and re-layouts  11.8 us

profile of v1, /device:TPU:0, one launch (start us, length us, event | category | flops | bytes accessed | tf_op | source)
XLA Modules:
  0.0 51.8 jit_solution(10499109927201026077)
XLA Ops:
  0.0 0.0 copy-start.9
  0.0 0.0 copy-start.12
  0.0 0.0 copy-start.14
  0.0 0.0 copy-start.11
  0.0 0.0 copy-start.13
  0.0 0.7 %copy-done.9 = bf16[31,128]{1,0:T(8,128)(2,1)S(1)} copy-done((bf16[31,128]{1,0:T(8,128)(2,1)S(1)}, bf16[31,128]{1,0:T(8,128)(2,1)}, u32[]{:S(2)}) %copy-start.9) | copy-done | bytes 7960
  0.7 0.0 copy-done.12
  0.7 0.0 copy-done.14
  0.7 0.0 copy-done.11
  0.7 0.0 copy-done.13
  0.7 0.0 copy-start
  0.7 1.0 %copy-done = bf16[1024,256]{1,0:T(8,128)(2,1)S(1)} copy-done((bf16[1024,256]{1,0:T(8,128)(2,1)S(1)}, bf16[1024,256]{1,0:T(8,128)(2,1)}, u32[]{:S(2)}) %copy-start) | copy-done | bytes 524312
  1.8 0.0 copy-start.1
  1.8 1.0 %copy-done.1 = bf16[1024,256]{1,0:T(8,128)(2,1)S(1)} copy-done((bf16[1024,256]{1,0:T(8,128)(2,1)S(1)}, bf16[1024,256]{1,0:T(8,128)(2,1)}, u32[]{:S(2)}) %copy-start.1) | copy-done | bytes 524312
  2.8 0.0 copy-start.2
  2.8 1.0 %copy-done.2 = bf16[1024,256]{1,0:T(8,128)(2,1)S(1)} copy-done((bf16[1024,256]{1,0:T(8,128)(2,1)S(1)}, bf16[1024,256]{1,0:T(8,128)(2,1)}, u32[]{:S(2)}) %copy-start.2) | copy-done | bytes 524312
  3.9 0.0 copy-start.3
  3.9 1.0 %copy-done.3 = bf16[1024,256]{1,0:T(8,128)(2,1)S(1)} copy-done((bf16[1024,256]{1,0:T(8,128)(2,1)S(1)}, bf16[1024,256]{1,0:T(8,128)(2,1)}, u32[]{:S(2)}) %copy-start.3) | copy-done | bytes 524312
  4.9 0.0 copy-start.4
  4.9 1.0 %copy-done.4 = bf16[256,1024]{1,0:T(8,128)(2,1)S(1)} copy-done((bf16[256,1024]{1,0:T(8,128)(2,1)S(1)}, bf16[256,1024]{1,0:T(8,128)(2,1)}, u32[]{:S(2)}) %copy-start.4) | copy-done | bytes 524312
  5.9 0.0 copy-start.5
  5.9 0.9 %copy-done.5 = bf16[1,128,1024]{2,1,0:T(8,128)(2,1)S(1)} copy-done((bf16[1,128,1024]{2,1,0:T(8,128)(2,1)S(1)}, bf16[1,128,1024]{2,1,0:T(8,128)(2,1)}, u32[]{:S(2)}) %copy-start.5) | copy-done | bytes 262168
  6.9 0.0 copy-start.6
  6.9 0.9 %copy-done.6 = bf16[1024,128]{1,0:T(8,128)(2,1)S(1)} copy-done((bf16[1024,128]{1,0:T(8,128)(2,1)S(1)}, bf16[1024,128]{1,0:T(8,128)(2,1)}, u32[]{:S(2)}) %copy-start.6) | copy-done | bytes 262168
  7.8 0.0 copy-start.7
  7.8 0.9 %copy-done.7 = bf16[1024,128]{1,0:T(8,128)(2,1)S(1)} copy-done((bf16[1024,128]{1,0:T(8,128)(2,1)S(1)}, bf16[1024,128]{1,0:T(8,128)(2,1)}, u32[]{:S(2)}) %copy-start.7) | copy-done | bytes 262168
  8.8 0.0 copy-start.8
  8.8 0.9 %copy-done.8 = bf16[128,1024]{1,0:T(8,128)(2,1)S(1)} copy-done((bf16[128,1024]{1,0:T(8,128)(2,1)S(1)}, bf16[128,1024]{1,0:T(8,128)(2,1)}, u32[]{:S(2)}) %copy-start.8) | copy-done | bytes 262168
  9.7 0.0 copy-start.10
  9.7 0.7 %copy-done.10 = f32[1024]{0:T(1024)S(1)} copy-done((f32[1024]{0:T(1024)S(1)}, f32[1024]{0:T(1024)}, u32[]{:S(2)}) %copy-start.10) | copy-done | bytes 4120
  10.4 0.0 copy-start.15
  10.4 0.7 %copy-done.15 = f32[128]{0:T(128)S(1)} copy-done((f32[128]{0:T(128)S(1)}, f32[128]{0:T(128)}, u32[]{:S(2)}) %copy-start.15) | copy-done | bytes 536
  11.1 40.0 %shard_map.154 = bf16[1,128,1024]{2,1,0:T(8,128)(2,1)S(1)} custom-call(bf16[1,128,1024]{2,1,0:T(8,128)(2,1)S(1)} %copy-done.5, f32[1,1024]{1,0:T(1,128)S(1)} %bitcast.6, bf16[1024,128]{1,0:T(8,128)(2,1)S(1)} %copy-done.6, bf16[1024,128]{1,0:T(8,128)(2,1)S(1)} %copy-done.7, bf16[31,128]{1,0:T(8,128)(2,1)S(1)} %copy-done.9, f32[1,128]{1,0:T(1,128)S(1)} %bitcast.9, ...), custom_call_target="tpu_custom_call" | custom-call | tf_op jit(solution)/shard_map/pallas_call | solution.py:410
  51.1 0.7 %copy.18 = bf16[1,128,1024]{2,1,0:T(8,128)(2,1)} copy(bf16[1,128,1024]{2,1,0:T(8,128)(2,1)S(1)} %shard_map.154) | data formatting | bytes 524288
Async XLA Ops:
  0.0 0.7 %copy-start.9 = (bf16[31,128]{1,0:T(8,128)(2,1)S(1)}, bf16[31,128]{1,0:T(8,128)(2,1)}, u32[]{:S(2)}) copy-start(bf16[31,128]{1,0:T(8,128)(2,1)} %taps.1) | copy-start | bytes 23812
  0.0 0.7 %copy-start.12 = (f32[256]{0:T(256)S(1)}, f32[256]{0:T(256)}, u32[]{:S(2)}) copy-start(f32[256]{0:T(256)} %param.29) | copy-start | bytes 3076
  0.0 0.7 %copy-start.14 = (f32[128]{0:T(128)S(1)}, f32[128]{0:T(128)}, u32[]{:S(2)}) copy-start(f32[128]{0:T(128)} %param.22) | copy-start | bytes 1540
  0.0 0.7 %copy-start.11 = (f32[256]{0:T(256)S(1)}, f32[256]{0:T(256)}, u32[]{:S(2)}) copy-start(f32[256]{0:T(256)} %param.28) | copy-start | bytes 3076
  0.0 0.7 %copy-start.13 = (f32[128]{0:T(128)S(1)}, f32[128]{0:T(128)}, u32[]{:S(2)}) copy-start(f32[128]{0:T(128)} %param.21) | copy-start | bytes 1540
  0.7 1.0 %copy-start = (bf16[1024,256]{1,0:T(8,128)(2,1)S(1)}, bf16[1024,256]{1,0:T(8,128)(2,1)}, u32[]{:S(2)}) copy-start(bf16[1024,256]{1,0:T(8,128)(2,1)} %qw.1) | copy-start | bytes 1572868
  1.8 1.0 %copy-start.1 = (bf16[1024,256]{1,0:T(8,128)(2,1)S(1)}, bf16[1024,256]{1,0:T(8,128)(2,1)}, u32[]{:S(2)}) copy-start(bf16[1024,256]{1,0:T(8,128)(2,1)} %fw.1) | copy-start | bytes 1572868
  2.8 1.0 %copy-start.2 = (bf16[1024,256]{1,0:T(8,128)(2,1)S(1)}, bf16[1024,256]{1,0:T(8,128)(2,1)}, u32[]{:S(2)}) copy-start(bf16[1024,256]{1,0:T(8,128)(2,1)} %iw.1) | copy-start | bytes 1572868
  3.9 1.0 %copy-start.3 = (bf16[1024,256]{1,0:T(8,128)(2,1)S(1)}, bf16[1024,256]{1,0:T(8,128)(2,1)}, u32[]{:S(2)}) copy-start(bf16[1024,256]{1,0:T(8,128)(2,1)} %gw.1) | copy-start | bytes 1572868
  4.9 1.0 %copy-start.4 = (bf16[256,1024]{1,0:T(8,128)(2,1)S(1)}, bf16[256,1024]{1,0:T(8,128)(2,1)}, u32[]{:S(2)}) copy-start(bf16[256,1024]{1,0:T(8,128)(2,1)} %row.1) | copy-start | bytes 1572868
  5.9 0.9 %copy-start.5 = (bf16[1,128,1024]{2,1,0:T(8,128)(2,1)S(1)}, bf16[1,128,1024]{2,1,0:T(8,128)(2,1)}, u32[]{:S(2)}) copy-start(bf16[1,128,1024]{2,1,0:T(8,128)(2,1)} %frames.1) | copy-start | bytes 786436
  6.9 0.9 %copy-start.6 = (bf16[1024,128]{1,0:T(8,128)(2,1)S(1)}, bf16[1024,128]{1,0:T(8,128)(2,1)}, u32[]{:S(2)}) copy-start(bf16[1024,128]{1,0:T(8,128)(2,1)} %cvw.1) | copy-start | bytes 786436
  7.8 0.9 %copy-start.7 = (bf16[1024,128]{1,0:T(8,128)(2,1)S(1)}, bf16[1024,128]{1,0:T(8,128)(2,1)}, u32[]{:S(2)}) copy-start(bf16[1024,128]{1,0:T(8,128)(2,1)} %cgw.1) | copy-start | bytes 786436
  8.8 0.9 %copy-start.8 = (bf16[128,1024]{1,0:T(8,128)(2,1)S(1)}, bf16[128,1024]{1,0:T(8,128)(2,1)}, u32[]{:S(2)}) copy-start(bf16[128,1024]{1,0:T(8,128)(2,1)} %cow.1) | copy-start | bytes 786436
  9.7 0.7 %copy-start.10 = (f32[1024]{0:T(1024)S(1)}, f32[1024]{0:T(1024)}, u32[]{:S(2)}) copy-start(f32[1024]{0:T(1024)} %param.17) | copy-start | bytes 12292
  10.4 0.7 %copy-start.15 = (f32[128]{0:T(128)S(1)}, f32[128]{0:T(128)}, u32[]{:S(2)}) copy-start(f32[128]{0:T(128)} %param.23) | copy-start | bytes 1540

commit v2 on v1

--- a/solution.py
+++ b/solution.py
@@ -36,8 +36,8 @@
     out,
     gath, wbuf, ow, norm_v, taps_v, cb_v, cg_v, cs_v, rate_v, hg_v,
     gated, edges, ext, filt, stat, stat_in, conv_send, conv_in, rec_send, rec_in,
-    grown_s, shrunk_s, value_s, gate_s, local_s, state, state_in, decay, decay_in, carry_out, carry_in, acc,
-    loc_sem, fr_send, fr_recv, ow_send, ow_recv, ed_send, ed_recv, stt_send, stt_recv, dc_send, dc_recv,
+    grown_s, shrunk_s, value_s, gate_s, local_s, state, state_in, carry_out, carry_in, acc,
+    loc_sem, fr_send, fr_recv, ow_send, ow_recv, ed_send, ed_recv, stt_send, stt_recv,
     ca_send, ca_recv, sm_send, sm_recv, cv_send, cv_recv, rc_send, rc_recv,
 ):
     n_tp, n_sp, spt, d_conv, seq_total = cfg
@@ -46,6 +46,8 @@
     conv_n, rec_n = cvw.shape[1], qw.shape[1]
     heads = rec_n // HEAD
     chunk = carry_out.shape[1]
+    groups = carry_out.shape[0] // n_sp
+    together = seqs // groups
     tp, sp = lax.axis_index("tp"), lax.axis_index("sp")
 
     barrier = pltpu.get_barrier_semaphore()
@@ -89,7 +91,11 @@
     pl.semaphore_wait(barrier, n_tp - 1 + n_sp - 1)
     for k in direct:
         fr[k].start()
-    for copy in copies:
+    for copy in copies[14:]:
+        copy.wait()
+    for k in direct:
+        wt[k].start()
+    for copy in copies[:14]:
         copy.wait()
 
     t_row = lax.broadcasted_iota(jnp.int32, (positions, positions), 0)
@@ -99,14 +105,45 @@
     lower3 = jnp.concatenate([lower, lower, lower], axis=1)
     rate_row = rate_v[...] / seq_total
 
-    sent_states = []
-
-    def state_copies(p):
-        pair = p * chunk // HEAD
-        return (
-            remote(state.at[pl.ds(p * chunk, chunk)], state_in.at[sp], stt_send.at[p], stt_recv.at[sp], sp=p),
-            remote(decay.at[pair], decay_in.at[sp], dc_send.at[p], dc_recv.at[sp], sp=p),
-        )
+    def state_copy(g, p):
+        n = g * n_sp + p
+        return remote(state.at[n], state_in.at[g * n_sp + sp], stt_send.at[n], stt_recv.at[g * n_sp + sp], sp=p)
+
+    def state_from(g, j):
+        n = g * n_sp + j
+        return remote(state.at[n], state_in.at[n], stt_send.at[n], stt_recv.at[n], sp=j)
+
+    def carry_copy(g, j):
+        n = g * n_sp + j
+        here = pl.multiple_of((g * n_sp + sp) * chunk, chunk)
+        return remote(carry_out.at[n], carry_in.at[pl.ds(here, chunk)], ca_send.at[n], ca_recv.at[g * n_sp + sp], sp=j)
+
+    def carry_from(g, j):
+        n = g * n_sp + j
+        return remote(carry_out.at[n], carry_in.at[pl.ds(n * chunk, chunk)], ca_send.at[n], ca_recv.at[n], sp=j)
+
+    def scan(g):
+        mine = g * n_sp + sp
+        state_in[mine] = state[mine]
+        carried = jnp.zeros((chunk, HEAD), F32)
+        for j in range(n_sp):
+            n = g * n_sp + j
+            carry_out[n] = carried.astype(BF16)
+            if j > 0:
+
+                @pl.when(sp != j)
+                def _():
+                    carry_copy(g, j).start()
+
+            if j < n_sp - 1:
+
+                @pl.when(sp != j)
+                def _():
+                    state_from(g, j).wait_recv()
+
+                carried = state_in[n, chunk : chunk + 1, :] * carried + state_in[n, 0:chunk, :]
+        here = pl.multiple_of(mine * chunk, chunk)
+        carry_in[pl.ds(here, chunk), :] = carry_out[mine]
 
     def edge_copy(q):
         return remote(
@@ -118,9 +155,6 @@
             fr[k].wait_recv()
             if k % 2 == 0:
                 fr[k + 1].start()
-        if k == min(2, n_tp - 1):
-            for j in direct:
-                wt[j].start()
         for i in range(spt):
             q = k * spt + i
             x = gath[k, i].astype(F32)
@@ -152,19 +186,26 @@
             for h in range(heads):
                 pair = q * heads + h
                 lanes = slice(h * HEAD, (h + 1) * HEAD)
-                state[pair * HEAD : (pair + 1) * HEAD] = mm(value[:, lanes], weighted[:, lanes], ((0,), (0,)))
-                decay[pair] = jnp.broadcast_to(last_decay[:, lanes], (8, HEAD))
-                for p in range(pair * HEAD // chunk, (pair + 1) * HEAD // chunk):
+                block = mm(value[:, lanes], weighted[:, lanes], ((0,), (0,)))
+                rows_decay = jnp.broadcast_to(last_decay[:, lanes], (8, HEAD))
+                for r in range(HEAD // chunk):
+                    n = pair * (HEAD // chunk) + r
+                    state[n, 0:chunk] = block[r * chunk : (r + 1) * chunk]
+                    state[n, chunk : chunk + 8] = rows_decay
+            if (q + 1) % together == 0:
+                g = q // together
+                for p in range(n_sp):
 
                     @pl.when(jnp.logical_and(sp != p, sp < n_sp - 1))
                     def _():
-                        for copy in state_copies(p):
-                            copy.start()
+                        state_copy(g, p).start()
 
             shrunk_s[q] = (in_gate * jnp.exp(-cumulative)).astype(BF16)
             queries = project(offsets[2], rec_n).astype(F32)
             grown_s[q] = (queries * jnp.exp(cumulative)).astype(BF16)
             gate_s[q] = project(offsets[5], rec_n)
+            if (q + 1) % together == 0 and q // together > 0:
+                scan(q // together - 1)
 
     reach = taps.shape[0] - 1
     for q in range(seqs):
@@ -188,37 +229,7 @@
     for k in range(1, n_tp):
         stat_copy(k).start()
 
-    own = pl.multiple_of(sp * chunk, chunk)
-    state_in[sp] = state[pl.ds(own, chunk), :]
-    decay_in[sp] = decay[sp * chunk // HEAD]
-
-    def carry_copy(j):
-        return remote(carry_out.at[j], carry_in.at[pl.ds(own, chunk)], ca_send.at[j], ca_recv.at[sp], sp=j)
-
-    def from_source(j):
-        return (
-            remote(state.at[pl.ds(0, chunk)], state_in.at[j], stt_send.at[j], stt_recv.at[j], sp=j),
-            remote(decay.at[0], decay_in.at[j], dc_send.at[j], dc_recv.at[j], sp=j),
-        )
-
-    carried = jnp.zeros((chunk, HEAD), F32)
-    for j in range(n_sp):
-        carry_out[j] = carried.astype(BF16)
-        if j > 0:
-
-            @pl.when(sp != j)
-            def _():
-                carry_copy(j).start()
-
-        if j < n_sp - 1:
-
-            @pl.when(sp != j)
-            def _():
-                for copy in from_source(j):
-                    copy.wait_recv()
-
-            carried = decay_in[j, 0:1, :] * carried + state_in[j]
-    carry_in[pl.ds(own, chunk), :] = carry_out[sp]
+    scan(groups - 1)
 
     for q in range(seqs):
         for h in range(heads):
@@ -258,22 +269,23 @@
         if k > 0:
             conv_copy(k).start()
 
-    for j in range(n_sp):
-
-        @pl.when(jnp.logical_and(sp != j, sp > 0))
-        def _():
-            remote(
-                carry_out.at[0], carry_in.at[pl.ds(j * chunk, chunk)], ca_send.at[j], ca_recv.at[j], sp=j
-            ).wait_recv()
-
     @pl.when(sp == 0)
     def _():
         carry_in[...] = jnp.zeros_like(carry_in)
 
-    for k in order:
+    arrived = set()
+    for k in [1, 0] + list(range(2, n_tp)):
         for i in range(spt):
             q = k * spt + i
             rows = slice(i * positions, (i + 1) * positions)
+            g = q // together
+            for j in range(n_sp if g not in arrived else 0):
+
+                @pl.when(jnp.logical_and(sp != j, sp > 0))
+                def _():
+                    carry_from(g, j).wait_recv()
+
+            arrived.add(g)
             for h in range(heads):
                 pair = q * heads + h
                 lanes = slice(h * HEAD, (h + 1) * HEAD)
@@ -320,18 +332,18 @@
         rec_copy(k).wait_send()
     for q in range(seqs):
         edge_copy(q).wait_send()
-    for p in range(n_sp):
-
-        @pl.when(jnp.logical_and(sp != p, sp < n_sp - 1))
-        def _():
-            for copy in state_copies(p):
-                copy.wait_send()
-
-        if p > 0:
-
-            @pl.when(sp != p)
+    for g in range(groups):
+        for p in range(n_sp):
+
+            @pl.when(jnp.logical_and(sp != p, sp < n_sp - 1))
             def _():
-                carry_copy(p).wait_send()
+                state_copy(g, p).wait_send()
+
+            if p > 0:
+
+                @pl.when(sp != p)
+                def _():
+                    carry_copy(g, p).wait_send()
 
 
 def wide(array, axis):
@@ -358,7 +370,12 @@
     seqs = n_tp * spt
     heads = rec_n // HEAD
     pairs = seqs * heads
-    chunk = pairs * HEAD // n_sp
+    together = 1
+    while together < seqs and together * heads * HEAD // n_sp < 16:
+        together *= 2
+    groups = seqs // together
+    chunk = together * heads * HEAD // n_sp
+    slots = groups * n_sp
     width = conv_n * 2 + rec_n * 4
     rows = spt * positions
     vm = pltpu.VMEM
@@ -389,20 +406,17 @@
         vm((seqs, positions, rec_n), BF16),
         vm((seqs, positions, rec_n), BF16),
         vm((seqs, positions, rec_n), F32),
-        vm((pairs * HEAD, HEAD), F32),
-        vm((n_sp, chunk, HEAD), F32),
-        vm((pairs, 8, HEAD), F32),
-        vm((n_sp, 8, HEAD), F32),
-        vm((n_sp, chunk, HEAD), BF16),
+        vm((slots, chunk + 8, HEAD), F32),
+        vm((slots, chunk + 8, HEAD), F32),
+        vm((slots, chunk, HEAD), BF16),
         vm((pairs * HEAD, HEAD), BF16),
         vm((rows, out_n), F32),
         sem((16,)),
         sem((n_tp,)), sem((n_tp,)),
         sem((n_tp,)), sem((n_tp,)),
         sem((seqs,)), sem((seqs,)),
-        sem((n_sp,)), sem((n_sp,)),
-        sem((n_sp,)), sem((n_sp,)),
-        sem((n_sp,)), sem((n_sp,)),
+        sem((slots,)), sem((slots,)),
+        sem((slots,)), sem((slots,)),
         sem((n_tp,)), sem((n_tp,)),
         sem((n_tp,)), sem((n_tp,)),
         sem((n_tp,)), sem((n_tp,)),
@@ -410,11 +424,11 @@
     return pl.pallas_call(
         functools.partial(kernel, (n_tp, n_sp, spt, d_conv, positions * n_sp)),
         out_shape=jax.ShapeDtypeStruct((spt, positions, out_n), BF16),
-        in_specs=[pl.BlockSpec(memory_space=pl.ANY)] * 16,
+        in_specs=[pl.BlockSpec(memory_space=pltpu.HBM)] * 16,
         out_specs=pl.BlockSpec(memory_space=pltpu.VMEM),
         scratch_shapes=scratch,
         compiler_params=pltpu.CompilerParams(
-            collective_id=0, has_side_effects=True, vmem_limit_bytes=48 * 1024 * 1024
+            collective_id=0, has_side_effects=True, vmem_limit_bytes=56 * 1024 * 1024
         ),
     )(
         frames, norm_gain[None], conv_value_w, conv_gate_w, conv_taps, conv_bias[None], channel_gain[None],

time: 52.4 us -> 41.6 us (0.79)
  local copies, waits for them, and re-layouts: 11.8 us -> 1.67 us
    unnamed x33 -> x1, local copies, waits for them, and re-layouts: 11.8 us -> 1.67 us
where the time goes in v2:
time: 41.6 us; the launch traced here: 41.5 us
  Pallas kernels  39.8 us (96%)
  local copies, waits for them, and re-layouts  1.67 us (4%)
    pallas_call x1, Pallas kernels, local(): pl.pallas_call(functools.partial(kernel, (n_tp, n_sp, spt, d_conv, positi...  39.8 us
    unnamed x1, local copies, waits for them, and re-layouts  1.67 us

profile of v2, /device:TPU:0, one launch (start us, length us, event | category | flops | bytes accessed | tf_op | source)
XLA Modules:
  0.0 41.5 jit_solution(13409016228274323758)
XLA Ops:
  0.0 39.8 %shard_map.154 = bf16[1,128,1024]{2,1,0:T(8,128)(2,1)} custom-call(bf16[1,128,1024]{2,1,0:T(8,128)(2,1)} %frames.1, f32[1,1024]{1,0:T(1,128)} %bitcast.6, bf16[1024,128]{1,0:T(8,128)(2,1)} %cvw.1, bf16[1024,128]{1,0:T(8,128)(2,1)} %cgw.1, bf16[31,128]{1,0:T(8,128)(2,1)} %taps.1, f32[1,128]{1,0:T(1,128)} %bitcast.9, f32[1,128]{1,0:T(1,128)} %bitcast.10, ...), custom_call_target="tpu_custom_call" | custom-call | tf_op jit(solution)/shard_map/pallas_call | solution.py:424
  39.8 1.7 %copy.18 = bf16[1,128,1024]{2,1,0:T(8,128)(2,1)} copy(bf16[1,128,1024]{2,1,0:T(8,128)(2,1)} %shard_map.154) | data formatting | bytes 524288

commit v3 on v2

--- a/solution.py
+++ b/solution.py
@@ -38,7 +38,7 @@
     gated, edges, ext, filt, stat, stat_in, conv_send, conv_in, rec_send, rec_in,
     grown_s, shrunk_s, value_s, gate_s, local_s, state, state_in, carry_out, carry_in, acc,
     loc_sem, fr_send, fr_recv, ow_send, ow_recv, ed_send, ed_recv, stt_send, stt_recv,
-    ca_send, ca_recv, sm_send, sm_recv, cv_send, cv_recv, rc_send, rc_recv,
+    ca_send, ca_recv, sm_send, sm_recv, cv_send, cv_recv, rc_send, rc_recv, wc_send, wc_recv,
 ):
     n_tp, n_sp, spt, d_conv, seq_total = cfg
     positions, depth = frames.shape[1], frames.shape[2]
@@ -87,6 +87,12 @@
     for k in range(1, n_tp):
         source, to = (0, k) if k in direct else (k - 1, 1)
         wt[k] = remote(ow.at[source], ow.at[k], ow_send.at[k], ow_recv.at[k], tp=flip(tp, to))
+
+    wc = {}
+    for k in range(2, n_tp, 2):
+        late, early = pl.ds(0, conv_n), pl.ds(conv_n, rec_n)
+        wt[k] = remote(ow.at[0, early], ow.at[k, early], ow_send.at[k], ow_recv.at[k], tp=flip(tp, k))
+        wc[k] = remote(ow.at[0, late], ow.at[k, late], wc_send.at[k], wc_recv.at[k], tp=flip(tp, k))
 
     pl.semaphore_wait(barrier, n_tp - 1 + n_sp - 1)
     for k in direct:
@@ -228,6 +234,8 @@
 
     for k in range(1, n_tp):
         stat_copy(k).start()
+    for k in wc:
+        wc[k].start()
 
     scan(groups - 1)
 
@@ -305,6 +313,7 @@
 
     for k in range(2, n_tp, 2):
         wt[k].wait_recv()
+        wc[k].wait_recv()
         wt[k + 1].start()
     if n_tp > 1:
         wt[1].wait_recv()
@@ -327,6 +336,8 @@
     for k in range(1, n_tp):
         fr[k].wait_send()
         wt[k].wait_send()
+        if k in wc:
+            wc[k].wait_send()
         stat_copy(k).wait_send()
         conv_copy(k).wait_send()
         rec_copy(k).wait_send()
@@ -420,6 +431,7 @@
         sem((n_tp,)), sem((n_tp,)),
         sem((n_tp,)), sem((n_tp,)),
         sem((n_tp,)), sem((n_tp,)),
+        sem((n_tp,)), sem((n_tp,)),
     ]
     return pl.pallas_call(
         functools.partial(kernel, (n_tp, n_sp, spt, d_conv, positions * n_sp)),

time: 41.6 us -> 40 us (0.962)
  Pallas kernels: 39.8 us -> 38.2 us
    pallas_call x1, Pallas kernels: 39.8 us -> 38.2 us  [local(): pl.pallas_call(functools.partial(kernel, (n_tp, n_sp, spt, d_conv, positi...]
where the time goes in v3:
time: 40 us; the launch traced here: 39.8 us
  Pallas kernels  38.2 us (96%)
  local copies, waits for them, and re-layouts  1.67 us (4%)
    pallas_call x1, Pallas kernels, local(): pl.pallas_call(functools.partial(kernel, (n_tp, n_sp, spt, d_conv, positi...  38.2 us
    unnamed x1, local copies, waits for them, and re-layouts  1.67 us

profile of v3, /device:TPU:0, one launch (start us, length us, event | category | flops | bytes accessed | tf_op | source)
XLA Modules:
  0.0 39.8 jit_solution(11979080011656976947)
XLA Ops:
  0.0 38.2 %shard_map.154 = bf16[1,128,1024]{2,1,0:T(8,128)(2,1)} custom-call(bf16[1,128,1024]{2,1,0:T(8,128)(2,1)} %frames.1, f32[1,1024]{1,0:T(1,128)} %bitcast.6, bf16[1024,128]{1,0:T(8,128)(2,1)} %cvw.1, bf16[1024,128]{1,0:T(8,128)(2,1)} %cgw.1, bf16[31,128]{1,0:T(8,128)(2,1)} %taps.1, f32[1,128]{1,0:T(1,128)} %bitcast.9, f32[1,128]{1,0:T(1,128)} %bitcast.10, ...), custom_call_target="tpu_custom_call" | custom-call | tf_op jit(solution)/shard_map/pallas_call | solution.py:436
  38.2 1.7 %copy.18 = bf16[1,128,1024]{2,1,0:T(8,128)(2,1)} copy(bf16[1,128,1024]{2,1,0:T(8,128)(2,1)} %shard_map.154) | data formatting | bytes 524288
